TPU v7x, 32 devices: a whole 2x2x4 slice. The times are simulated.
32 devices in a mesh: sp: 8 (over z, x), tp: 4 (over y, core).
Axes of the slice: x: 2, y: 2, z: 4, core: 2. Of those that a mesh axis runs over, the one named last changes fastest.
Arguments:
- glu_a: bfloat16 [2048, 1024], P('sp', 'tp'), may hold values from -6 to 6
- glu_b: bfloat16 [2048, 1024], P('sp', 'tp'), may hold values from -6 to 6
- saved_conv: bfloat16 [2048, 1024], P('sp', 'tp')
- taps: float32 [31, 1024], P(None, 'tp'), may hold values from -1 to 1
- norm_gain_vector: float32 [1024], P('tp'), may hold values from 0.1 to 1.9
- out_proj: bfloat16 [1024, 2048], P('tp'), may hold values from -0.1875 to 0.1875
- moe_in: bfloat16 [2048, 2048], P('sp'), may hold values from -6 to 6
- grad_out: bfloat16 [2048, 2048], P('sp'), may hold values from -6 to 6
- expert_ids: int32 [2048, 2], P('sp'), may hold values from 0 to 7, all different within a row; in each aligned block of 256 rows (0 to 255, 256 to 511, ...) at most 96 rows name the same one
- route_weights: float32 [2048, 2], P('sp'), may hold values from 0.3 to 2
- w_gate: bfloat16 [8, 2048, 1024], P('sp', None, 'tp'), may hold values from -0.125 to 0.125
- w_up: bfloat16 [8, 2048, 1024], P('sp', None, 'tp'), may hold values from -0.125 to 0.125
- w_down: bfloat16 [8, 1024, 2048], P('sp', 'tp'), may hold values from -0.1875 to 0.1875
Outputs:
- grad_glu_a: bfloat16 [2048, 1024], P('sp', 'tp')
- grad_glu_b: bfloat16 [2048, 1024], P('sp', 'tp')
- grad_out_proj: float32 [2048, 1024], P('sp', 'tp')
- grad_gate: bfloat16 [8, 2048, 1024], P('sp', None, 'tp')
- grad_up: bfloat16 [8, 2048, 1024], P('sp', None, 'tp')
- grad_down: bfloat16 [8, 1024, 2048], P('sp', 'tp')
Inputs may be any that keep to these rules, and one draw needn't show every extreme that they name: `expert_ids`: in each aligned block of 256 tokens, a token's 2 experts differ, and no expert is named more than 96 times; some expert reaches 96 in some blocks.
All inputs are finite; a program needn't handle non-finite values.
Results may differ from a plain program's by a relative error of at most 0.015.
Values may be sent and summed in bfloat16 or wider, within the bound.
A program may use at most 64 MiB of HBM per device.

v0:
```python
import jax
import jax.numpy as jnp
from jax import lax
from jax.sharding import PartitionSpec as P

CONV_CHANNELS = 1024


def with_halo(array, sides, width):
    for axis, dim in sides:
        size, length = (lax.axis_size(axis), array.shape[dim])
        up = [(i, (i + 1) % size) for i in range(size - 1)]
        down = [(j, i) for i, j in up]
        last = lax.slice_in_dim(array, length - width, length, axis=dim)
        initial = lax.slice_in_dim(array, 0, width, axis=dim)
        before = lax.ppermute(last, axis, up)
        after = lax.ppermute(initial, axis, down)
        array = jnp.concatenate([before, array, after], axis=dim)
    return array


def expert_local(in_rows, cot_rows, w_gate, w_up, w_down):
    gate_pre = jnp.einsum("esd,edf->esf", in_rows, w_gate, preferred_element_type=jnp.float32)
    up_pre = jnp.einsum("esd,edf->esf", in_rows, w_up, preferred_element_type=jnp.float32)
    sig_gate = jax.nn.sigmoid(gate_pre)
    act_gate = gate_pre * sig_gate
    hidden = (act_gate * up_pre).astype(jnp.bfloat16)
    grad_hidden = jnp.einsum("esd,efd->esf", cot_rows, w_down, preferred_element_type=jnp.float32)
    grad_upact = (grad_hidden * act_gate).astype(jnp.bfloat16)
    grad_gateact = (grad_hidden * up_pre * sig_gate * (1.0 + gate_pre * (1.0 - sig_gate))).astype(
        jnp.bfloat16
    )
    return (hidden, grad_upact, grad_gateact)


def weight_grads(in_rows, cot_rows, hidden, grad_upact, grad_gateact):
    grad_down = jnp.einsum(
        "esf,esd->efd", hidden, cot_rows, preferred_element_type=jnp.float32
    ).astype(jnp.bfloat16)
    grad_gate = jnp.einsum(
        "esd,esf->edf", in_rows, grad_gateact, preferred_element_type=jnp.float32
    ).astype(jnp.bfloat16)
    grad_up = jnp.einsum(
        "esd,esf->edf", in_rows, grad_upact, preferred_element_type=jnp.float32
    ).astype(jnp.bfloat16)
    return (grad_gate, grad_up, grad_down)


def per_device(
    glu_a,
    glu_b,
    saved_conv,
    taps,
    norm_gain_vector,
    out_proj,
    moe_in,
    grad_out,
    expert_ids,
    route_weights,
    w_gate,
    w_up,
    w_down,
):
    n_sp = lax.axis_size("sp")
    n_tp = lax.axis_size("tp")
    tp_pos = lax.axis_index("tp")
    tok_dev, d_model = grad_out.shape
    top_count = expert_ids.shape[1]
    exp_dev = w_gate.shape[0]
    experts = exp_dev * n_sp
    capacity = max(2, 3 * tok_dev * top_count // (2 * experts))
    quarter = d_model // n_tp
    pair_count = tok_dev * top_count
    flat_ids = expert_ids.reshape(pair_count)
    onehot = (flat_ids[:, None] == jnp.arange(experts, dtype=jnp.int32)[None, :]).astype(jnp.int32)
    slot_rank = jnp.sum((jnp.cumsum(onehot, axis=0) - onehot) * onehot, axis=1)
    slot_of = flat_ids * capacity + slot_rank
    owner_idx = (
        jnp.full((experts * capacity,), pair_count, jnp.int32)
        .at[slot_of]
        .set(jnp.arange(pair_count, dtype=jnp.int32))
    )
    token_idx = owner_idx // top_count
    scaled = (grad_out.astype(jnp.float32)[:, None, :] * route_weights[:, :, None]).astype(
        jnp.bfloat16
    )
    scaled = scaled.reshape(pair_count, d_model)

    def to_expert(rows):
        width = rows.shape[1]
        return (
            rows.reshape(n_sp, exp_dev, capacity, width)
            .swapaxes(0, 1)
            .reshape(exp_dev, n_sp * capacity, width)
        )

    in_part = lax.dynamic_slice_in_dim(moe_in, tp_pos * quarter, quarter, 1)
    cot_part = lax.dynamic_slice_in_dim(scaled, tp_pos * quarter, quarter, 1)
    in_pad = jnp.concatenate([in_part, jnp.zeros((1, quarter), jnp.bfloat16)], axis=0)
    cot_pad = jnp.concatenate([cot_part, jnp.zeros((1, quarter), jnp.bfloat16)], axis=0)
    sent_in, sent_cot = (
        lax.all_to_all(in_pad[token_idx], "sp", split_axis=0, concat_axis=0, tiled=True),
        lax.all_to_all(cot_pad[owner_idx], "sp", split_axis=0, concat_axis=0, tiled=True),
    )
    recv_in, recv_cot = (
        lax.all_gather(sent_in, "tp", axis=1, tiled=True),
        lax.all_gather(sent_cot, "tp", axis=1, tiled=True),
    )
    in_rows = to_expert(recv_in)
    cot_rows = to_expert(recv_cot)
    hidden, grad_upact, grad_gateact = expert_local(in_rows, cot_rows, w_gate, w_up, w_down)
    grad_gate, grad_up, grad_down = weight_grads(
        in_rows, cot_rows, hidden, grad_upact, grad_gateact
    )
    partial_value = jnp.einsum(
        "esf,edf->esd", grad_gateact, w_gate, preferred_element_type=jnp.float32
    )
    partial_value = partial_value + jnp.einsum(
        "esf,edf->esd", grad_upact, w_up, preferred_element_type=jnp.float32
    )
    partial_value = partial_value.astype(jnp.bfloat16)
    row_grads = (
        lax.psum_scatter(partial_value, "tp", scatter_dimension=2, tiled=True)
        .astype(jnp.float32)
        .astype(jnp.bfloat16)
    )
    row_grads = (
        row_grads.reshape(exp_dev, n_sp, capacity, quarter)
        .swapaxes(0, 1)
        .reshape(n_sp * exp_dev * capacity, quarter)
    )
    returned = lax.all_to_all(row_grads, "sp", split_axis=0, concat_axis=0, tiled=True)
    picked = returned[slot_of].reshape(tok_dev, top_count, quarter).astype(jnp.float32)
    grad_own = lax.dynamic_slice_in_dim(grad_out, tp_pos * quarter, quarter, 1).astype(jnp.float32)
    mix_part = (grad_own + jnp.sum(picked, axis=1)).astype(jnp.bfloat16)
    grad_mix = lax.all_gather(mix_part, "tp", axis=1, tiled=True)
    head_gradient = lax.dot_general(
        grad_mix, out_proj, (((1,), (1,)), ((), ())), preferred_element_type=jnp.float32
    )
    convolved_rows = saved_conv.astype(jnp.float32)
    sum_c, sum_sq = lax.psum(
        (jnp.sum(convolved_rows, axis=1), jnp.sum(convolved_rows * convolved_rows, axis=1)), "tp"
    )
    channel_average = (sum_c / CONV_CHANNELS)[:, None]
    var_c = (sum_sq / CONV_CHANNELS)[:, None] - channel_average * channel_average
    inverse_deviation = lax.rsqrt(var_c + 1e-05)
    centered_scaled = (convolved_rows - channel_average) * inverse_deviation
    normalized_rows = centered_scaled * norm_gain_vector[None, :]
    sigmoid_of_norm = jax.nn.sigmoid(normalized_rows)
    heads = (normalized_rows * sigmoid_of_norm).astype(jnp.bfloat16)
    grad_out_proj = lax.psum_scatter(
        lax.dot_general(
            grad_mix, heads, (((0,), (0,)), ((), ())), preferred_element_type=jnp.float32
        ),
        "sp",
        scatter_dimension=0,
        tiled=True,
    )
    normalized_gradient = (
        head_gradient
        * sigmoid_of_norm
        * (1.0 + normalized_rows * (1.0 - sigmoid_of_norm))
        * norm_gain_vector[None, :]
    )
    gradient_total, product_total = lax.psum(
        (
            jnp.sum(normalized_gradient, axis=1),
            jnp.sum(normalized_gradient * centered_scaled, axis=1),
        ),
        "tp",
    )
    convolved_gradient = (
        inverse_deviation
        * (
            normalized_gradient
            - (gradient_total / CONV_CHANNELS)[:, None]
            - centered_scaled * (product_total / CONV_CHANNELS)[:, None]
        )
    ).astype(jnp.bfloat16)
    reach = (taps.shape[0] - 1) // 2
    padded = with_halo(convolved_gradient, (("sp", 0),), reach).astype(jnp.float32)
    grad_y = jnp.zeros(head_gradient.shape, jnp.float32)
    for tap_idx in range(taps.shape[0]):
        grad_y = (
            grad_y
            + taps[tap_idx][None, :] * padded[2 * reach - tap_idx : 2 * reach - tap_idx + tok_dev]
        )
    sig_b = jax.nn.sigmoid(glu_b.astype(jnp.float32))
    grad_glu_a = (grad_y * sig_b).astype(jnp.bfloat16)
    grad_glu_b = (grad_y * glu_a.astype(jnp.float32) * sig_b * (1.0 - sig_b)).astype(jnp.bfloat16)
    return (grad_glu_a, grad_glu_b, grad_out_proj, grad_gate, grad_up, grad_down)


def solution(mesh):
    in_specs = (
        P("sp", "tp"),
        P("sp", "tp"),
        P("sp", "tp"),
        P(None, "tp"),
        P("tp"),
        P("tp", None),
        P("sp", None),
        P("sp", None),
        P("sp", None),
        P("sp", None),
        P("sp", None, "tp"),
        P("sp", None, "tp"),
        P("sp", "tp", None),
    )
    out_specs = (
        P("sp", "tp"),
        P("sp", "tp"),
        P("sp", "tp"),
        P("sp", None, "tp"),
        P("sp", None, "tp"),
        P("sp", "tp", None),
    )
    return jax.shard_map(
        per_device, mesh=mesh, in_specs=in_specs, out_specs=out_specs, check_vma=False
    )
```

profile of v0, /device:TPU:0, one launch (start us, length us, event | category | flops | bytes accessed | tf_op | source)
XLA Modules:
  0.0 280.5 jit_solution(9579719425612122031)
XLA Ops:
  10.9 2.4 scatter_custom_fusion
  14.4 2.7 gather_fusion.1
  17.1 27.3 %all_to_all.36 = bf16[8,96,512]{2,1,0:T(8,128)(2,1)} all-to-all(bf16[8,96,512]{2,1,0:T(8,128)(2,1)S(1)} %bitcast.85), channel_id=1, replica_groups=mesh['sp'=8,'tp'=4] {'sp'}, dimensions={0} | all-to-all | bytes 1572864 | tf_op jit(solution)/shard_map/all_to_all | solution.py:102
  44.8 4.1 %mul.456 = f32[256,2,2048]{2,1,0:T(2,128)} broadcast(bf16[256,2048]{1,0:T(8,128)(2,1)S(1)} %copy-done.1), dimensions={0,2} | broadcast | bytes 5242880 | tf_op jit(solution)/shard_map/mul | solution.py:84
  48.9 6.4 %mul.457 = f32[512,2048]{1,0:T(8,128)} reshape(f32[256,2,2048]{2,1,0:T(2,128)} %mul.456) | data formatting | bytes 8388608 | tf_op jit(solution)/shard_map/mul | solution.py:84
  56.7 2.7 gather_fusion
  59.4 23.1 %all_to_all.37 = bf16[8,96,512]{2,1,0:T(8,128)(2,1)} all-to-all(bf16[8,96,512]{2,1,0:T(8,128)(2,1)S(1)} %bitcast.86), channel_id=1, replica_groups=mesh['sp'=8,'tp'=4] {'sp'}, dimensions={0} | all-to-all | bytes 1572864 | tf_op jit(solution)/shard_map/all_to_all | solution.py:103
  82.7 3.9 %fusion.9 = f32[768,256]{1,0:T(8,128)} fusion(bf16[768,2048]{1,0:T(8,128)(2,1)} %all-gather.6.cloned.1.call-done, bf16[1,2048,256]{2,1,0:T(8,128)(2,1)S(1)} %copy-done), kind=kOutput, calls=%fused_computation.19 | convolution fusion | flops 805306368 | bytes 4980736 | tf_op jit(solution)/shard_map/esd,edf->esf/dot_general | solution.py:23
  88.5 21.8 %all-gather.4.cloned.1.call-done = bf16[768,2048]{1,0:T(8,128)(2,1)} async-done(((bf16[768,512]{1,0:T(8,128)(2,1)}), bf16[768,2048]{1,0:T(8,128)(2,1)}) %all-gather.4.cloned.1.call-update) | async-done | bytes 3145744 | tf_op jit(solution)/shard_map/all_gather | solution.py:107
  110.3 3.8 %multiply_convert_fusion.1 = (bf16[768,256]{1,0:T(8,128)(2,1)S(1)}, bf16[768,256]{1,0:T(8,128)(2,1)S(1)}) fusion(f32[768,256]{1,0:T(8,128)} %fusion.9, f32[768,256]{1,0:T(8,128)} %fusion.12, bf16[768,2048]{1,0:T(8,128)(2,1)} %all-gather.4.cloned.1.call-done, bf16[1,256,2048]{2,1,0:T(8,128)(2,1)} %param.25), kind=kOutput, calls=%fused_computation.27 | convolution fusion | flops 807862272 | bytes 6553600 | tf_op jit(solution)/shard_map/esd,efd->esf/dot_general | solution.py:28
  115.1 2.7 fusion
  117.9 37.9 %reduce-scatter.3.cloned.1.call-done = bf16[1,768,512]{2,1,0:T(8,128)(2,1)} async-done(((bf16[1,768,2048]{2,1,0:T(8,128)(2,1)}), bf16[1,768,512]{2,1,0:T(8,128)(2,1)}) %reduce-scatter.3.cloned.1.call-update) | async-done | bytes 786448 | tf_op jit(solution)/shard_map/reduce_scatter | solution.py:123
  155.8 5.5 %all-to-all-start.2 = ((bf16[8,96,512]{2,1,0:T(8,128)(2,1)}), bf16[8,96,512]{2,1,0:T(8,128)(2,1)S(1)}, u32[]{:S(2)}, u32[]{:S(2)}) async-start(bf16[8,96,512]{2,1,0:T(8,128)(2,1)} %bitcast.89), calls=%async_computation.3 | async-start | bytes 1572864 | tf_op jit(solution)/shard_map/all_to_all | solution.py:132
  161.5 19.8 %all-to-all-done.2 = bf16[8,96,512]{2,1,0:T(8,128)(2,1)S(1)} async-done(((bf16[8,96,512]{2,1,0:T(8,128)(2,1)}), bf16[8,96,512]{2,1,0:T(8,128)(2,1)S(1)}, u32[]{:S(2)}, u32[]{:S(2)}) %all-to-all-start.2) | async-done | bytes 786464 | tf_op jit(solution)/shard_map/all_to_all | solution.py:132
  181.4 2.0 gather_fusion.2
  187.2 5.9 %all-reduce.3 = (f32[256]{0:T(256)S(1)}, f32[256]{0:T(256)S(1)}) all-reduce(f32[256]{0:T(256)S(1)} %get-tuple-element.9, f32[256]{0:T(256)S(1)} %get-tuple-element.8), channel_id=1, replica_groups=mesh['sp'=8,'tp'=4] {'tp'}, use_global_device_ids=true, to_apply=%region_3.4 | all-reduce | flops 512 | bytes 4096 | tf_op jit(solution)/shard_map/psum | solution.py:141
  193.2 8.7 %all-gather.8.cloned.1.call-done = bf16[256,2048]{1,0:T(8,128)(2,1)} async-done(((bf16[256,512]{1,0:T(8,128)(2,1)}), bf16[256,2048]{1,0:T(8,128)(2,1)}) %all-gather.8.cloned.1.call-update) | async-done | bytes 1048592 | tf_op jit(solution)/shard_map/all_gather | solution.py:136
  201.9 3.2 %fusion.65 = f32[2048,256]{1,0:T(8,128)} fusion(bf16[256,2048]{1,0:T(8,128)(2,1)} %all-gather.8.cloned.1.call-done, bf16[256,256]{1,0:T(8,128)(2,1)S(1)} %copy-done.2, f32[256]{0:T(256)S(1)} %copy-done.9, f32[256]{0:T(256)S(1)} %get-tuple-element.54, f32[256]{0:T(256)S(1)} %get-tuple-element.53), kind=kOutput, calls=%fused_computation.117 | convolution fusion | flops 269025280 | bytes 3279872 | tf_op jit(solution)/shard_map/dot_general | solution.py:152
  205.1 4.0 %fusion.2 = bf16[1,2048,256]{2,1,0:T(8,128)(2,1)} fusion(bf16[768,2048]{1,0:T(8,128)(2,1)} %all-gather.6.cloned.1.call-done, bf16[768,256]{1,0:T(8,128)(2,1)S(1)} %get-tuple-element.16), kind=kOutput, calls=%fused_computation.10 | convolution fusion | flops 805830656 | bytes 4587520 | tf_op jit(solution)/shard_map/esd,esf->edf/dot_general | solution.py:43
  209.2 2.0 fusion.3
  211.8 6.3 %all-reduce.2 = (f32[256]{0:T(256)S(1)}, f32[256]{0:T(256)S(1)}) all-reduce(f32[256]{0:T(256)S(1)} %get-tuple-element.7, f32[256]{0:T(256)S(1)} %get-tuple-element.6), channel_id=1, replica_groups=mesh['sp'=8,'tp'=4] {'tp'}, use_global_device_ids=true, to_apply=%region_13.14 | all-reduce | flops 512 | bytes 4096 | tf_op jit(solution)/shard_map/psum | solution.py:165
  218.4 3.5 %collective-permute-start = (bf16[15,256]{1,0:T(8,128)(2,1)S(1)}, bf16[15,256]{1,0:T(8,128)(2,1)S(1)}, u32[]{:S(2)}, u32[]{:S(2)}) collective-permute-start(bf16[15,256]{1,0:T(8,128)(2,1)S(1)} %get-tuple-element.18), channel_id=1, source_target_pairs={{0,4},{4,8},{8,12},{12,16},{16,20},{20,24},{24,28},{1,5},{5,9},{9,... | collective-permute-start | bytes 23048 | tf_op jit(solution)/shard_map/ppermute | solution.py:16
  223.4 3.9 %fusion.1 = bf16[1,2048,256]{2,1,0:T(8,128)(2,1)} fusion(bf16[768,2048]{1,0:T(8,128)(2,1)} %all-gather.6.cloned.1.call-done, bf16[768,256]{1,0:T(8,128)(2,1)S(1)} %get-tuple-element.17), kind=kOutput, calls=%fused_computation.9 | convolution fusion | flops 805830656 | bytes 4587520 | tf_op jit(solution)/shard_map/esd,esf->edf/dot_general | solution.py:40
  230.0 44.0 %reduce-scatter.5.cloned.1.call-done = f32[256,256]{1,0:T(8,128)} async-done(((f32[2048,256]{1,0:T(8,128)}), f32[256,256]{1,0:T(8,128)}) %reduce-scatter.5.cloned.1.call-update) | async-done | bytes 262160 | tf_op jit(solution)/shard_map/reduce_scatter | solution.py:151
  (84 shorter events, 18.6 us)
Async XLA Ops:
  7.2 75.5 %copy-start = (bf16[1,2048,256]{2,1,0:T(8,128)(2,1)S(1)}, bf16[1,2048,256]{2,1,0:T(8,128)(2,1)}, u32[]{:S(2)}) copy-start(bf16[1,2048,256]{2,1,0:T(8,128)(2,1)} %param.23) | copy-start | bytes 3145732
  7.2 75.5 %all-gather.6.cloned.1.call-start = ((), (), s32[]{:S(2)}) async-start(), calls=%async_computation.6 | async-start | bytes 3932160 | tf_op jit(solution)/shard_map/all_gather | solution.py:106
  14.4 30.1 %copy-start.8 = (f32[256,2]{0,1:T(2,128)S(1)}, f32[256,2]{0,1:T(2,128)}, u32[]{:S(2)}) copy-start(f32[256,2]{0,1:T(2,128)} %param.22) | copy-start | bytes 6148
  14.4 30.4 %copy-start.1 = (bf16[256,2048]{1,0:T(8,128)(2,1)S(1)}, bf16[256,2048]{1,0:T(8,128)(2,1)}, u32[]{:S(2)}) copy-start(bf16[256,2048]{1,0:T(8,128)(2,1)} %param.20) | copy-start | bytes 3145732
  44.5 65.8 %all-gather.4.cloned.1.call-start = ((), (), s32[]{:S(2)}) async-start(), calls=%async_computation.5 | async-start | bytes 3932160 | tf_op jit(solution)/shard_map/all_gather | solution.py:107
  82.6 4.0 %copy-start.4 = (bf16[1,2048,256]{2,1,0:T(8,128)(2,1)S(1)}, bf16[1,2048,256]{2,1,0:T(8,128)(2,1)}, u32[]{:S(2)}) copy-start(bf16[1,2048,256]{2,1,0:T(8,128)(2,1)} %param.24) | copy-start | bytes 3145732
  82.6 73.1 %reduce-scatter.3.cloned.1.call-start = ((), (), s32[]{:S(2)}) async-start(), calls=%async_computation.7 | async-start | bytes 3932160 | tf_op jit(solution)/shard_map/reduce_scatter | solution.py:123
  82.7 3.9 %copy-start.10 = (bf16[768,2048]{1,0:T(8,128)(2,1)S(1)}, bf16[768,2048]{1,0:T(8,128)(2,1)}, u32[]{:S(2)}) copy-start(bf16[768,2048]{1,0:T(8,128)(2,1)} %all-gather.6.cloned.1.call-done) | copy-start | bytes 9437188
  155.8 25.6 %all-to-all-start.2 = ((bf16[8,96,512]{2,1,0:T(8,128)(2,1)}), bf16[8,96,512]{2,1,0:T(8,128)(2,1)S(1)}, u32[]{:S(2)}, u32[]{:S(2)}) async-start(bf16[8,96,512]{2,1,0:T(8,128)(2,1)} %bitcast.89), calls=%async_computation.3 | async-start | bytes 1572864 | tf_op jit(solution)/shard_map/all_to_all | solution.py:132
  161.3 40.6 %all-gather.8.cloned.1.call-start = ((), (), s32[]{:S(2)}) async-start(), calls=%async_computation.8 | async-start | bytes 1310720 | tf_op jit(solution)/shard_map/all_gather | solution.py:136
  183.3 3.7 %copy-start.2 = (bf16[256,256]{1,0:T(8,128)(2,1)S(1)}, bf16[256,256]{1,0:T(8,128)(2,1)}, u32[]{:S(2)}) copy-start(bf16[256,256]{1,0:T(8,128)(2,1)} %param.15) | copy-start | bytes 393220
  183.3 18.5 %copy-start.9 = (f32[256]{0:T(256)S(1)}, f32[256]{0:T(256)}, u32[]{:S(2)}) copy-start(f32[256]{0:T(256)} %param.17) | copy-start | bytes 3076
  187.0 18.1 %copy-start.7 = (f32[31,256]{1,0:T(8,128)S(1)}, f32[31,256]{1,0:T(8,128)}, u32[]{:S(2)}) copy-start(f32[31,256]{1,0:T(8,128)} %param.16) | copy-start | bytes 95236
  187.0 87.0 %reduce-scatter.5.cloned.1.call-start = ((), (), s32[]{:S(2)}) async-start(), calls=%async_computation.9 | async-start | bytes 2359296 | tf_op jit(solution)/shard_map/reduce_scatter | solution.py:151
  205.1 4.1 %copy-start.11 = (bf16[768,2048]{1,0:T(8,128)(2,1)S(1)}, bf16[768,2048]{1,0:T(8,128)(2,1)}, u32[]{:S(2)}) copy-start(bf16[768,2048]{1,0:T(8,128)(2,1)} %all-gather.4.cloned.1.call-done) | copy-start | bytes 9437188
  205.1 4.1 %copy-start.13 = (f32[768,256]{1,0:T(8,128)S(1)}, f32[768,256]{1,0:T(8,128)}, u32[]{:S(2)}) copy-start(f32[768,256]{1,0:T(8,128)} %fusion.9) | copy-start | bytes 2359300
  205.1 4.1 %copy-start.14 = (f32[768,256]{1,0:T(8,128)S(1)}, f32[768,256]{1,0:T(8,128)}, u32[]{:S(2)}) copy-start(f32[768,256]{1,0:T(8,128)} %fusion.12) | copy-start | bytes 2359300
  209.2 2.1 copy-start.3
  209.2 2.0 copy-start.12
  218.4 8.9 %collective-permute-start = (bf16[15,256]{1,0:T(8,128)(2,1)S(1)}, bf16[15,256]{1,0:T(8,128)(2,1)S(1)}, u32[]{:S(2)}, u32[]{:S(2)}) collective-permute-start(bf16[15,256]{1,0:T(8,128)(2,1)S(1)} %get-tuple-element.18), channel_id=1, source_target_pairs={{0,4},{4,8},{8,12},{12,16},{16,20},{20,24},{24,28},{1,5},{5,9},{9,... | collective-permute-start | bytes 23048 | tf_op jit(solution)/shard_map/ppermute | solution.py:16
  221.9 5.8 %copy-start.5 = (bf16[256,256]{1,0:T(8,128)(2,1)S(1)}, bf16[256,256]{1,0:T(8,128)(2,1)}, u32[]{:S(2)}) copy-start(bf16[256,256]{1,0:T(8,128)(2,1)} %param.14) | copy-start | bytes 393220
  221.9 5.8 %copy-start.6 = (bf16[256,256]{1,0:T(8,128)(2,1)S(1)}, bf16[256,256]{1,0:T(8,128)(2,1)}, u32[]{:S(2)}) copy-start(bf16[256,256]{1,0:T(8,128)(2,1)} %param.13) | copy-start | bytes 393220
  221.9 5.7 %collective-permute-start.1 = (bf16[15,256]{1,0:T(8,128)(2,1)S(1)}, bf16[15,256]{1,0:T(8,128)(2,1)S(1)}, u32[]{:S(2)}, u32[]{:S(2)}) collective-permute-start(bf16[15,256]{1,0:T(8,128)(2,1)S(1)} %get-tuple-element.19), channel_id=1, source_target_pairs={{4,0},{8,4},{12,8},{16,12},{20,16},{24,20},{28,24},{5,1},{9,5},{13... | collective-permute-start | bytes 23048 | tf_op jit(solution)/shard_map/ppermute | solution.py:17
Sparse Core Ops, SparseCore 0:
  44.6 27.5 all-gather.5
  82.7 27.5 all-gather.3
  118.0 37.7 reduce-scatter.2
  187.1 14.6 all-gather.7
  205.8 68.1 reduce-scatter.4
where the time goes:
time: 281 us
  waiting for transfers between devices  133 us (47%)
  blocking collectives  62.7 us (22%)
  matrix products  27.1 us (10%)
  local copies, waits for them, and re-layouts  23.9 us (9%)
  between operations  14.2 us (5%)
  starting transfers between devices  10.8 us (4%)
  other arithmetic  9.13 us (3%)
    reduce_scatter x1, waiting for transfers between devices, per_device(): lax.psum_scatter(lax.dot_general(grad_mix, heads, (((0,), (0,)), ((), ())...  44 us
    reduce_scatter x1, waiting for transfers between devices, per_device(): lax.psum_scatter(partial_value, 'tp', scatter_dimension=2, tiled=True)  37.9 us
    all_to_all x1, blocking collectives, per_device(): lax.all_to_all(in_pad[token_idx], 'sp', split_axis=0, concat_axis=0, tile...  27.3 us
    all_to_all x1, blocking collectives, per_device(): lax.all_to_all(cot_pad[owner_idx], 'sp', split_axis=0, concat_axis=0, til...  23.1 us
    all_gather x1, waiting for transfers between devices, per_device(): lax.all_gather(sent_cot, 'tp', axis=1, tiled=True)  21.8 us
    all_to_all x1, waiting for transfers between devices, per_device(): lax.all_to_all(row_grads, 'sp', split_axis=0, concat_axis=0, tiled=True)  19.8 us
    mul x3, local copies, waits for them, and re-layouts, per_device(): grad_out.astype(jnp.float32)[:, None, :] * route_weights[:, :, None]  10.6 us
    all_gather x1, waiting for transfers between devices, per_device(): grad_mix = lax.all_gather(mix_part, 'tp', axis=1, tiled=True)  8.7 us
  transfers between devices with their start and end apart: 8, of which 6 were waited for; matrix products, arithmetic and copies ran while one was open for 12% of the time, Pallas kernels for 0%

commit v1 on v0

--- a/solution.py
+++ b/solution.py
@@ -4,6 +4,13 @@
 from jax.sharding import PartitionSpec as P
 
 CONV_CHANNELS = 1024
+
+
+def gather_over(x, axis, along):
+    count = lax.axis_size(axis)
+    shards = jnp.stack([x for _ in range(count)])
+    shards = lax.all_to_all(shards, axis, split_axis=0, concat_axis=0)
+    return jnp.concatenate(shards, axis=along)
 
 
 def with_halo(array, sides, width):
@@ -104,7 +111,7 @@
     )
     recv_in, recv_cot = (
         lax.all_gather(sent_in, "tp", axis=1, tiled=True),
-        lax.all_gather(sent_cot, "tp", axis=1, tiled=True),
+        gather_over(sent_cot, "tp", 1),
     )
     in_rows = to_expert(recv_in)
     cot_rows = to_expert(recv_cot)

time: 281 us -> 295 us (1.050)
  waiting for transfers between devices: 133 us -> 138 us
  starting transfers between devices: 10.8 us -> 15.5 us
    all_to_all x0 -> x1, waiting for transfers between devices: none -> 31.1 us  [gather_over(): shards = lax.all_to_all(shards, axis, split_axis=0, concat_axis=0)]
    all_gather x1 -> x0, waiting for transfers between devices: 21.8 us -> none  [per_device(): lax.all_gather(sent_cot, 'tp', axis=1, tiled=True)]
    all_to_all x0 -> x1, starting transfers between devices: none -> 4.65 us  [gather_over(): shards = lax.all_to_all(shards, axis, split_axis=0, concat_axis=0)]
  transfers between devices with their start and end apart: 8 -> 8, of which waited for: 6 -> 6; matrix products, arithmetic and copies ran while one was open for 12% -> 13% of each run, Pallas kernels for 0% -> 0%
where the time goes in v1:
time: 295 us
  waiting for transfers between devices  138 us (47%)
  blocking collectives  62.6 us (21%)
  matrix products  29.1 us (10%)
  local copies, waits for them, and re-layouts  26.1 us (9%)
  starting transfers between devices  15.5 us (5%)
  between operations  14.2 us (5%)
  other arithmetic  9.13 us (3%)
    reduce_scatter x1, waiting for transfers between devices, per_device(): lax.psum_scatter(lax.dot_general(grad_mix, heads, (((0,), (0,)), ((), ())...  42.1 us
    reduce_scatter x1, waiting for transfers between devices, per_device(): lax.psum_scatter(partial_value, 'tp', scatter_dimension=2, tiled=True)  35.9 us
    all_to_all x1, waiting for transfers between devices, gather_over(): shards = lax.all_to_all(shards, axis, split_axis=0, concat_axis=0)  31.1 us
    all_to_all x1, blocking collectives, per_device(): lax.all_to_all(in_pad[token_idx], 'sp', split_axis=0, concat_axis=0, tile...  27.3 us
    all_to_all x1, blocking collectives, per_device(): lax.all_to_all(cot_pad[owner_idx], 'sp', split_axis=0, concat_axis=0, til...  23 us
    all_to_all x1, waiting for transfers between devices, per_device(): lax.all_to_all(row_grads, 'sp', split_axis=0, concat_axis=0, tiled=True)  19.8 us
    mul x3, local copies, waits for them, and re-layouts, per_device(): grad_out.astype(jnp.float32)[:, None, :] * route_weights[:, :, None]  10.7 us
    all_gather x1, waiting for transfers between devices, per_device(): grad_mix = lax.all_gather(mix_part, 'tp', axis=1, tiled=True)  8.67 us
  transfers between devices with their start and end apart: 8, of which 6 were waited for; matrix products, arithmetic and copies ran while one was open for 13% of the time, Pallas kernels for 0%

profile of v1, /device:TPU:0, one launch (start us, length us, event | category | flops | bytes accessed | tf_op | source)
XLA Modules:
  0.0 294.6 jit_solution(11963395521060101775)
XLA Ops:
  10.9 2.4 scatter_custom_fusion
  14.4 2.7 gather_fusion.1
  17.1 27.3 %all_to_all.38 = bf16[8,96,512]{2,1,0:T(8,128)(2,1)} all-to-all(bf16[8,96,512]{2,1,0:T(8,128)(2,1)S(1)} %bitcast.88), channel_id=1, replica_groups=mesh['sp'=8,'tp'=4] {'sp'}, dimensions={0} | all-to-all | bytes 1572864 | tf_op jit(solution)/shard_map/all_to_all | solution.py:109
  44.8 4.1 %mul.456 = f32[256,2,2048]{2,1,0:T(2,128)} broadcast(bf16[256,2048]{1,0:T(8,128)(2,1)S(1)} %copy-done.1), dimensions={0,2} | broadcast | bytes 5242880 | tf_op jit(solution)/shard_map/mul | solution.py:91
  48.9 6.4 %mul.457 = f32[512,2048]{1,0:T(8,128)} reshape(f32[256,2,2048]{2,1,0:T(2,128)} %mul.456) | data formatting | bytes 8388608 | tf_op jit(solution)/shard_map/mul | solution.py:91
  56.7 2.7 gather_fusion
  59.4 23.0 %all_to_all.39 = bf16[8,96,512]{2,1,0:T(8,128)(2,1)S(1)} all-to-all(bf16[8,96,512]{2,1,0:T(8,128)(2,1)S(1)} %bitcast.89), channel_id=1, replica_groups=mesh['sp'=8,'tp'=4] {'sp'}, dimensions={0} | all-to-all | bytes 1572864 | tf_op jit(solution)/shard_map/all_to_all | solution.py:110
  84.6 4.6 %all-to-all-start.1 = ((bf16[4,768,512]{1,2,0:T(8,128)(2,1)}), bf16[4,768,512]{1,2,0:T(8,128)(2,1)}, u32[]{:S(2)}, u32[]{:S(2)}) async-start(bf16[4,768,512]{1,2,0:T(8,128)(2,1)} %stack.10), calls=%async_computation.1 | async-start | bytes 6291456 | tf_op jit(solution)/shard_map/all_to_all | solution.py:12
  89.4 3.9 %fusion.9 = f32[768,256]{1,0:T(8,128)} fusion(bf16[768,2048]{1,0:T(8,128)(2,1)} %all-gather.3.cloned.1.call-done, bf16[1,2048,256]{2,1,0:T(8,128)(2,1)S(1)} %copy-done), kind=kOutput, calls=%fused_computation.19 | convolution fusion | flops 805306368 | bytes 4980736 | tf_op jit(solution)/shard_map/esd,edf->esf/dot_general | solution.py:30
  95.1 31.1 %all-to-all-done.1 = bf16[4,768,512]{1,2,0:T(8,128)(2,1)} async-done(((bf16[4,768,512]{1,2,0:T(8,128)(2,1)}), bf16[4,768,512]{1,2,0:T(8,128)(2,1)}, u32[]{:S(2)}, u32[]{:S(2)}) %all-to-all-start.1) | async-done | bytes 3145760 | tf_op jit(solution)/shard_map/all_to_all | solution.py:12
  126.2 3.8 %multiply_convert_fusion.1 = (bf16[768,256]{1,0:T(8,128)(2,1)S(1)}, bf16[768,256]{1,0:T(8,128)(2,1)S(1)}) fusion(f32[768,256]{1,0:T(8,128)} %fusion.9, f32[768,256]{1,0:T(8,128)} %fusion.12, bf16[768,2048]{0,1:T(8,128)(2,1)} %bitcast.8, bf16[1,256,2048]{2,1,0:T(8,128)(2,1)} %param.25), kind=kOutput, calls=%fused_computation.27 | convolution fusion | flops 807862272 | bytes 6553600 | tf_op jit(solution)/shard_map/esd,efd->esf/dot_general | solution.py:35
  131.0 2.7 fusion
  133.8 35.9 %reduce-scatter.3.cloned.1.call-done = bf16[1,768,512]{2,1,0:T(8,128)(2,1)} async-done(((bf16[1,768,2048]{2,1,0:T(8,128)(2,1)}), bf16[1,768,512]{2,1,0:T(8,128)(2,1)}) %reduce-scatter.3.cloned.1.call-update) | async-done | bytes 786448 | tf_op jit(solution)/shard_map/reduce_scatter | solution.py:130
  169.7 5.5 %all-to-all-start.3 = ((bf16[8,96,512]{2,1,0:T(8,128)(2,1)}), bf16[8,96,512]{2,1,0:T(8,128)(2,1)S(1)}, u32[]{:S(2)}, u32[]{:S(2)}) async-start(bf16[8,96,512]{2,1,0:T(8,128)(2,1)} %bitcast.92), calls=%async_computation.4 | async-start | bytes 1572864 | tf_op jit(solution)/shard_map/all_to_all | solution.py:139
  175.5 19.8 %all-to-all-done.3 = bf16[8,96,512]{2,1,0:T(8,128)(2,1)S(1)} async-done(((bf16[8,96,512]{2,1,0:T(8,128)(2,1)}), bf16[8,96,512]{2,1,0:T(8,128)(2,1)S(1)}, u32[]{:S(2)}, u32[]{:S(2)}) %all-to-all-start.3) | async-done | bytes 786464 | tf_op jit(solution)/shard_map/all_to_all | solution.py:139
  201.2 5.9 %all-reduce.3 = (f32[256]{0:T(256)S(1)}, f32[256]{0:T(256)S(1)}) all-reduce(f32[256]{0:T(256)S(1)} %get-tuple-element.9, f32[256]{0:T(256)S(1)} %get-tuple-element.8), channel_id=1, replica_groups=mesh['sp'=8,'tp'=4] {'tp'}, use_global_device_ids=true, to_apply=%region_3.4 | all-reduce | flops 512 | bytes 4096 | tf_op jit(solution)/shard_map/psum | solution.py:148
  207.1 8.7 %all-gather.5.cloned.1.call-done = bf16[256,2048]{1,0:T(8,128)(2,1)} async-done(((bf16[256,512]{1,0:T(8,128)(2,1)}), bf16[256,2048]{1,0:T(8,128)(2,1)}) %all-gather.5.cloned.1.call-update) | async-done | bytes 1048592 | tf_op jit(solution)/shard_map/all_gather | solution.py:143
  215.8 3.2 %fusion.65 = f32[2048,256]{1,0:T(8,128)} fusion(bf16[256,2048]{1,0:T(8,128)(2,1)} %all-gather.5.cloned.1.call-done, bf16[256,256]{1,0:T(8,128)(2,1)S(1)} %copy-done.2, f32[256]{0:T(256)S(1)} %copy-done.9, f32[256]{0:T(256)S(1)} %get-tuple-element.54, f32[256]{0:T(256)S(1)} %get-tuple-element.53), kind=kOutput, calls=%fused_computation.117 | convolution fusion | flops 269025280 | bytes 3279872 | tf_op jit(solution)/shard_map/dot_general | solution.py:159
  219.1 4.0 %fusion.2 = bf16[1,2048,256]{2,1,0:T(8,128)(2,1)} fusion(bf16[768,2048]{1,0:T(8,128)(2,1)} %all-gather.3.cloned.1.call-done, bf16[768,256]{1,0:T(8,128)(2,1)S(1)} %get-tuple-element.16), kind=kOutput, calls=%fused_computation.10 | convolution fusion | flops 805830656 | bytes 4587520 | tf_op jit(solution)/shard_map/esd,esf->edf/dot_general | solution.py:50
  223.1 4.1 %fusion.3 = bf16[1,256,2048]{2,1,0:T(8,128)(2,1)} fusion(bf16[768,2048]{0,1:T(8,128)(2,1)} %bitcast.8, f32[768,256]{1,0:T(8,128)S(1)} %copy-done.13, f32[768,256]{1,0:T(8,128)S(1)} %copy-done.12), kind=kOutput, calls=%fused_computation.11 | convolution fusion | flops 807010304 | bytes 5767168 | tf_op jit(solution)/shard_map/esf,esd->efd/dot_general | solution.py:44
  227.8 6.3 %all-reduce.2 = (f32[256]{0:T(256)S(1)}, f32[256]{0:T(256)S(1)}) all-reduce(f32[256]{0:T(256)S(1)} %get-tuple-element.7, f32[256]{0:T(256)S(1)} %get-tuple-element.6), channel_id=1, replica_groups=mesh['sp'=8,'tp'=4] {'tp'}, use_global_device_ids=true, to_apply=%region_13.14 | all-reduce | flops 512 | bytes 4096 | tf_op jit(solution)/shard_map/psum | solution.py:172
  234.3 3.5 %collective-permute-start = (bf16[15,256]{1,0:T(8,128)(2,1)S(1)}, bf16[15,256]{1,0:T(8,128)(2,1)S(1)}, u32[]{:S(2)}, u32[]{:S(2)}) collective-permute-start(bf16[15,256]{1,0:T(8,128)(2,1)S(1)} %get-tuple-element.18), channel_id=1, source_target_pairs={{0,4},{4,8},{8,12},{12,16},{16,20},{20,24},{24,28},{1,5},{5,9},{9,... | collective-permute-start | bytes 23048 | tf_op jit(solution)/shard_map/ppermute | solution.py:23
  239.3 4.0 %fusion.1 = bf16[1,2048,256]{2,1,0:T(8,128)(2,1)} fusion(bf16[768,2048]{1,0:T(8,128)(2,1)} %all-gather.3.cloned.1.call-done, bf16[768,256]{1,0:T(8,128)(2,1)S(1)} %get-tuple-element.17), kind=kOutput, calls=%fused_computation.9 | convolution fusion | flops 805830656 | bytes 4587520 | tf_op jit(solution)/shard_map/esd,esf->edf/dot_general | solution.py:47
  245.9 42.1 %reduce-scatter.5.cloned.1.call-done = f32[256,256]{1,0:T(8,128)} async-done(((f32[2048,256]{1,0:T(8,128)}), f32[256,256]{1,0:T(8,128)}) %reduce-scatter.5.cloned.1.call-update) | async-done | bytes 262160 | tf_op jit(solution)/shard_map/reduce_scatter | solution.py:158
  (83 shorter events, 22.5 us)
Async XLA Ops:
  7.2 82.2 %copy-start = (bf16[1,2048,256]{2,1,0:T(8,128)(2,1)S(1)}, bf16[1,2048,256]{2,1,0:T(8,128)(2,1)}, u32[]{:S(2)}) copy-start(bf16[1,2048,256]{2,1,0:T(8,128)(2,1)} %param.23) | copy-start | bytes 3145732
  7.2 82.2 %all-gather.3.cloned.1.call-start = ((), (), s32[]{:S(2)}) async-start(), calls=%async_computation.6 | async-start | bytes 3932160 | tf_op jit(solution)/shard_map/all_gather | solution.py:113
  14.4 30.1 %copy-start.8 = (f32[256,2]{0,1:T(2,128)S(1)}, f32[256,2]{0,1:T(2,128)}, u32[]{:S(2)}) copy-start(f32[256,2]{0,1:T(2,128)} %param.22) | copy-start | bytes 6148
  14.4 30.4 %copy-start.1 = (bf16[256,2048]{1,0:T(8,128)(2,1)S(1)}, bf16[256,2048]{1,0:T(8,128)(2,1)}, u32[]{:S(2)}) copy-start(bf16[256,2048]{1,0:T(8,128)(2,1)} %param.20) | copy-start | bytes 3145732
  84.6 41.6 %all-to-all-start.1 = ((bf16[4,768,512]{1,2,0:T(8,128)(2,1)}), bf16[4,768,512]{1,2,0:T(8,128)(2,1)}, u32[]{:S(2)}, u32[]{:S(2)}) async-start(bf16[4,768,512]{1,2,0:T(8,128)(2,1)} %stack.10), calls=%async_computation.1 | async-start | bytes 6291456 | tf_op jit(solution)/shard_map/all_to_all | solution.py:12
  89.3 4.0 %copy-start.4 = (bf16[1,2048,256]{2,1,0:T(8,128)(2,1)S(1)}, bf16[1,2048,256]{2,1,0:T(8,128)(2,1)}, u32[]{:S(2)}) copy-start(bf16[1,2048,256]{2,1,0:T(8,128)(2,1)} %param.24) | copy-start | bytes 3145732
  89.3 80.5 %reduce-scatter.3.cloned.1.call-start = ((), (), s32[]{:S(2)}) async-start(), calls=%async_computation.7 | async-start | bytes 3932160 | tf_op jit(solution)/shard_map/reduce_scatter | solution.py:130
  89.3 3.9 %copy-start.10 = (bf16[768,2048]{1,0:T(8,128)(2,1)S(1)}, bf16[768,2048]{1,0:T(8,128)(2,1)}, u32[]{:S(2)}) copy-start(bf16[768,2048]{1,0:T(8,128)(2,1)} %all-gather.3.cloned.1.call-done) | copy-start | bytes 9437188
  169.7 25.6 %all-to-all-start.3 = ((bf16[8,96,512]{2,1,0:T(8,128)(2,1)}), bf16[8,96,512]{2,1,0:T(8,128)(2,1)S(1)}, u32[]{:S(2)}, u32[]{:S(2)}) async-start(bf16[8,96,512]{2,1,0:T(8,128)(2,1)} %bitcast.92), calls=%async_computation.4 | async-start | bytes 1572864 | tf_op jit(solution)/shard_map/all_to_all | solution.py:139
  175.2 40.6 %all-gather.5.cloned.1.call-start = ((), (), s32[]{:S(2)}) async-start(), calls=%async_computation.8 | async-start | bytes 1310720 | tf_op jit(solution)/shard_map/all_gather | solution.py:143
  197.3 3.7 %copy-start.2 = (bf16[256,256]{1,0:T(8,128)(2,1)S(1)}, bf16[256,256]{1,0:T(8,128)(2,1)}, u32[]{:S(2)}) copy-start(bf16[256,256]{1,0:T(8,128)(2,1)} %param.15) | copy-start | bytes 393220
  197.3 18.5 %copy-start.9 = (f32[256]{0:T(256)S(1)}, f32[256]{0:T(256)}, u32[]{:S(2)}) copy-start(f32[256]{0:T(256)} %param.17) | copy-start | bytes 3076
  200.9 18.1 %copy-start.7 = (f32[31,256]{1,0:T(8,128)S(1)}, f32[31,256]{1,0:T(8,128)}, u32[]{:S(2)}) copy-start(f32[31,256]{1,0:T(8,128)} %param.16) | copy-start | bytes 95236
  201.0 87.1 %reduce-scatter.5.cloned.1.call-start = ((), (), s32[]{:S(2)}) async-start(), calls=%async_computation.9 | async-start | bytes 2359296 | tf_op jit(solution)/shard_map/reduce_scatter | solution.py:158
  219.1 4.0 %copy-start.12 = (f32[768,256]{1,0:T(8,128)S(1)}, f32[768,256]{1,0:T(8,128)}, u32[]{:S(2)}) copy-start(f32[768,256]{1,0:T(8,128)} %fusion.9) | copy-start | bytes 2359300
  219.1 4.0 %copy-start.13 = (f32[768,256]{1,0:T(8,128)S(1)}, f32[768,256]{1,0:T(8,128)}, u32[]{:S(2)}) copy-start(f32[768,256]{1,0:T(8,128)} %fusion.12) | copy-start | bytes 2359300
  223.1 4.1 %copy-start.3 = (bf16[256,2048]{1,0:T(8,128)(2,1)S(1)}, bf16[256,2048]{1,0:T(8,128)(2,1)}, u32[]{:S(2)}) copy-start(bf16[256,2048]{1,0:T(8,128)(2,1)} %all-gather.5.cloned.1.call-done) | copy-start | bytes 3145732
  223.1 4.1 %copy-start.11 = (bf16[256,2048]{1,0:T(8,128)(2,1)S(1)}, bf16[256,2048]{1,0:T(8,128)(2,1)}, u32[]{:S(2)}) copy-start(bf16[256,2048]{1,0:T(8,128)(2,1)} %param.18) | copy-start | bytes 3145732
  234.3 9.0 %collective-permute-start = (bf16[15,256]{1,0:T(8,128)(2,1)S(1)}, bf16[15,256]{1,0:T(8,128)(2,1)S(1)}, u32[]{:S(2)}, u32[]{:S(2)}) collective-permute-start(bf16[15,256]{1,0:T(8,128)(2,1)S(1)} %get-tuple-element.18), channel_id=1, source_target_pairs={{0,4},{4,8},{8,12},{12,16},{16,20},{20,24},{24,28},{1,5},{5,9},{9,... | collective-permute-start | bytes 23048 | tf_op jit(solution)/shard_map/ppermute | solution.py:23
  237.8 5.7 %copy-start.5 = (bf16[256,256]{1,0:T(8,128)(2,1)S(1)}, bf16[256,256]{1,0:T(8,128)(2,1)}, u32[]{:S(2)}) copy-start(bf16[256,256]{1,0:T(8,128)(2,1)} %param.14) | copy-start | bytes 393220
  237.9 5.7 %copy-start.6 = (bf16[256,256]{1,0:T(8,128)(2,1)S(1)}, bf16[256,256]{1,0:T(8,128)(2,1)}, u32[]{:S(2)}) copy-start(bf16[256,256]{1,0:T(8,128)(2,1)} %param.13) | copy-start | bytes 393220
  237.9 5.7 %collective-permute-start.1 = (bf16[15,256]{1,0:T(8,128)(2,1)S(1)}, bf16[15,256]{1,0:T(8,128)(2,1)S(1)}, u32[]{:S(2)}, u32[]{:S(2)}) collective-permute-start(bf16[15,256]{1,0:T(8,128)(2,1)S(1)} %get-tuple-element.19), channel_id=1, source_target_pairs={{4,0},{8,4},{12,8},{16,12},{20,16},{24,20},{28,24},{5,1},{9,5},{13... | collective-permute-start | bytes 23048 | tf_op jit(solution)/shard_map/ppermute | solution.py:24
Sparse Core Ops, SparseCore 0:
  44.6 27.5 all-gather.2
  133.9 35.7 reduce-scatter.2
  201.1 14.6 all-gather.4
  219.8 68.2 reduce-scatter.4
